TPU v7x, 32 devices: a whole 2x2x4 slice. The times are simulated.
32 devices in a mesh: sp: 4 (over z), fs: 4 (over y, x), tp: 2 (over core).
Axes of the slice: x: 2, y: 2, z: 4, core: 2. Of those that a mesh axis runs over, the one named last changes fastest.
Arguments:
- tokens: bfloat16 [4, 2048, 2048], P('fs', 'sp', 'tp'), may hold values from -6 to 6
- norm_gain: float32 [2048], replicated, may hold values from 0.1 to 1.9
- query_weight: bfloat16 [2048, 1024], P(('sp', 'fs'), 'tp'), may hold values from -0.125 to 0.125
- key_weight: bfloat16 [2048, 1024], P(('sp', 'fs'), 'tp'), may hold values from -0.125 to 0.125
- value_weight: bfloat16 [2048, 2048], P(('sp', 'fs'), 'tp'), may hold values from -0.125 to 0.125
- outgate_weight: bfloat16 [2048, 2048], P(('sp', 'fs'), 'tp'), may hold values from -0.125 to 0.125
- gate_weight: bfloat16 [2048, 2, 16], P(('sp', 'fs'), None, 'tp'), may hold values from -6 to 6
- forget_bias: float32 [16], P('tp')
- forget_shift: float32 [4, 16, 2048], P('fs', 'tp', 'sp'), may hold values from -1.5 to 0
- head_norm_gain: float32 [2048], P('tp'), may hold values from 0.1 to 1.9
- exit_weight: bfloat16 [2048, 2048], P(('sp', 'fs'), 'tp'), may hold values from -0.125 to 0.125
- entry_weight: bfloat16 [2048, 2048], P(('sp', 'fs'), 'tp'), may hold values from -0.125 to 0.125
- signal_weight: bfloat16 [2048, 2048], P(('sp', 'fs'), 'tp'), may hold values from -0.125 to 0.125
- conv_kernel: float32 [3, 2048], P(None, 'tp'), may hold values from -3.5 to 3.5
- merge_weight: bfloat16 [4096, 2048], P(('sp', 'fs'), 'tp'), may hold values from -0.09375 to 0.09375
Outputs:
- mixed: bfloat16 [4, 2048, 2048], P('fs', 'sp', 'tp')
All inputs are finite; a program needn't handle non-finite values.
Results may differ from a plain program's by a relative error of at most 0.017.
The roundings to bfloat16 on the way count: a program that leaves them out, or rounds other values in their place, can miss the bound.
Values may be sent and summed in bfloat16 or wider, within the bound.
A program may use at most 128 MiB of HBM per device.

v0:
```python
import jax
import jax.numpy as jnp
from jax import lax
from jax.experimental import pallas as pl
from jax.experimental.pallas import tpu as pltpu
from jax.sharding import PartitionSpec as P

DK = 64
DV = 128
BLOCK = 128
KERNEL = 3


EPSILON = 1e-06
EMPTY_LOG = -1e30
HIGHEST = lax.Precision.HIGHEST


def prefix(part, axis, combine, identity):
    place = lax.axis_index(axis)
    gathered = jax.tree.map(lambda a: lax.all_gather(a, axis), part)
    state = jax.tree.map(lambda a, e: jnp.zeros_like(a) + jnp.asarray(e, a.dtype), part, identity)

    def one(step, state):
        return combine(
            state, jax.tree.map(lambda a: lax.dynamic_index_in_dim(a, step, 0, False), gathered)
        )

    return lax.fori_loop(0, place, one, state)


def passed_along(value, axis, steps):
    count = lax.axis_size(axis)
    initial, last = (max(0, -steps), min(count, count - steps))
    return lax.ppermute(value, axis, [(source, source + steps) for source in range(initial, last)])


def combine(earlier, later):
    ceiling = jnp.maximum(later[2] + earlier[1], later[1])
    kept = jnp.exp(later[2] + earlier[1] - ceiling)
    added = jnp.exp(later[1] - ceiling)
    state = kept[..., None, None] * earlier[0] + added[..., None, None] * later[0]
    return (state, ceiling, earlier[2] + later[2])


def identity_state(heads):
    return (
        jnp.zeros((heads, DK, DV), jnp.float32),
        jnp.full((heads,), EMPTY_LOG, jnp.float32),
        jnp.zeros((heads,), jnp.float32),
    )


def add_product(left, piece):
    return jnp.dot(left, piece, preferred_element_type=jnp.float32)


def split_columns(total, stack):
    outputs = []
    offset = 0
    for weight in stack:
        outputs.append(total[:, offset : offset + weight.shape[1]])
        offset = offset + weight.shape[1]
    return outputs


def incoming_state(running):
    heads = running[1].shape[0]
    before = prefix((running[0], running[1], running[2]), "sp", combine, identity_state(heads))
    ceiling = jnp.maximum(before[1], before[2])
    shrink = jnp.exp(before[1] - ceiling)
    return (before[0] * shrink[:, None, None], ceiling, before[2])


def memory_states(keys, values, gates, forget_bias, forget_shift):
    count = gates.shape[0]
    heads = forget_bias.shape[0]
    blocks = count // BLOCK
    inputs = gates[:, :heads].reshape(blocks, BLOCK, heads)
    logs = jax.nn.log_sigmoid(gates[:, heads:] + forget_bias) + forget_shift[0].T
    cumulative = jnp.cumsum(logs.reshape(blocks, BLOCK, heads), axis=1)
    last = cumulative[:, -1]
    weight_logs = last[:, None, :] - cumulative + inputs
    peak = jnp.max(weight_logs, axis=1)
    coefficient_array = jnp.exp(weight_logs - peak[:, None, :])
    scaled = keys.reshape(blocks, BLOCK, heads, DK).astype(jnp.float32) * DK ** (-0.5)
    value_float = values.reshape(blocks, BLOCK, heads, DV).astype(jnp.float32)
    states = jnp.einsum(
        "csh,cshk,cshv->chkv", coefficient_array, scaled, value_float, precision=HIGHEST
    )
    running = identity_state(heads)
    prefixes = []
    for index in range(blocks):
        prefixes.append(running)
        running = combine(running, (states[index], peak[index], last[index]))
    leading_part = tuple((jnp.stack([item[member] for item in prefixes]) for member in range(3)))
    gate_apertures = combine(incoming_state(running), leading_part)
    return (gate_apertures, cumulative, inputs)


def memory_output(
    queries, keys, values, outgates, inputs, cumulative, gate_apertures, head_norm_gain
):
    blocks = cumulative.shape[0]
    heads = cumulative.shape[2]
    count = queries.shape[0]
    query_blocks = queries.reshape(blocks, BLOCK, heads, DK)
    key_blocks = keys.reshape(blocks, BLOCK, heads, DK)
    value_blocks = values.reshape(blocks, BLOCK, heads, DV)
    score_matrix = jnp.einsum(
        "cjhk,cshk->chjs", query_blocks, key_blocks, preferred_element_type=jnp.float32
    ) * DK ** (-0.5)
    cum_lanes = cumulative.transpose(0, 2, 1)
    input_lanes = inputs.transpose(0, 2, 1)
    causal = jnp.tril(jnp.ones((BLOCK, BLOCK), dtype=bool))
    decay = jnp.where(
        causal,
        cum_lanes[..., :, None] - cum_lanes[..., None, :] + input_lanes[..., None, :],
        -jnp.inf,
    )
    inter = cum_lanes + gate_apertures[1][..., None]
    ceiling = jnp.maximum(inter, jnp.max(decay, axis=-1))
    weighted = score_matrix * jnp.exp(decay - ceiling[..., None])
    numerator = jnp.einsum(
        "chjs,cshv->chjv",
        weighted.astype(jnp.bfloat16),
        value_blocks,
        preferred_element_type=jnp.float32,
    )
    query_float = query_blocks.astype(jnp.float32)
    carried = jnp.exp(inter - ceiling)
    numerator = numerator + carried[..., None] * jnp.einsum(
        "cjhk,chkv->chjv", query_float, gate_apertures[0], precision=HIGHEST
    )
    result = numerator * lax.rsqrt(
        jnp.mean(numerator * numerator, axis=-1, keepdims=True) + EPSILON
    )
    result = result.transpose(0, 2, 1, 3).reshape(count, heads * DV) * head_norm_gain
    return (result * jax.nn.sigmoid(outgates.astype(jnp.float32))).astype(jnp.bfloat16)


def local(
    tokens,
    norm_gain,
    query_weight,
    key_weight,
    value_weight,
    outgate_weight,
    gate_weight,
    forget_bias,
    forget_shift,
    head_norm_gain,
    exit_weight,
    entry_weight,
    signal_weight,
    conv_kernel,
    merge_weight,
):
    whole = lax.all_gather(tokens, "tp", axis=2, tiled=True)[0]
    count = whole.shape[0]
    flat = whole.astype(jnp.float32)
    normed = (
        flat * lax.rsqrt(jnp.mean(flat * flat, axis=-1, keepdims=True) + EPSILON) * norm_gain
    ).astype(jnp.bfloat16)
    gate_rows = gate_weight.reshape(gate_weight.shape[0], -1)
    state_stack = [key_weight, value_weight, gate_rows]
    other_stack = [query_weight, outgate_weight, exit_weight, entry_weight, signal_weight]
    stacked = jnp.concatenate(state_stack + other_stack, axis=1)
    total = add_product(normed, lax.all_gather(stacked, ("sp", "fs"), axis=0, tiled=True))
    columns = split_columns(total, state_stack + other_stack)
    keys = columns[0].astype(jnp.bfloat16)
    values = columns[1].astype(jnp.bfloat16)
    gate_apertures, cumulative, inputs = memory_states(
        keys, values, columns[2], forget_bias, forget_shift
    )
    others = columns[3:]
    queries = others[0].astype(jnp.bfloat16)
    outgates = others[1].astype(jnp.bfloat16)
    exit_rows = others[2].astype(jnp.bfloat16)
    entry_rows = others[3].astype(jnp.bfloat16)
    signal_rows = others[4].astype(jnp.bfloat16)
    mixed_in = (entry_rows.astype(jnp.float32) * signal_rows.astype(jnp.float32)).astype(
        jnp.bfloat16
    )
    rim = passed_along(mixed_in[count - (KERNEL - 1) :], "sp", 1)
    padded = jnp.concatenate([rim, mixed_in], axis=0).astype(jnp.float32)
    response = conv_kernel[0] * padded[0:count]
    for tap in range(1, KERNEL):
        response = response + conv_kernel[tap] * padded[tap : tap + count]
    conv_out = (exit_rows.astype(jnp.float32) * response).astype(jnp.bfloat16)
    memory_out = memory_output(
        queries, keys, values, outgates, inputs, cumulative, gate_apertures, head_norm_gain
    )
    memory_all, conv_all = (
        lax.all_gather(memory_out, "tp", axis=1, tiled=True),
        lax.all_gather(conv_out, "tp", axis=1, tiled=True),
    )
    concatenated_result = jnp.concatenate([memory_all, conv_all], axis=1)
    mixed = add_product(
        concatenated_result, lax.all_gather(merge_weight, ("sp", "fs"), axis=0, tiled=True)
    )
    return mixed.astype(jnp.bfloat16)[None]


def whole_states(keys, values, inputs, logs, blocks):
    heads = inputs.shape[1]
    inputs = inputs.reshape(blocks, BLOCK, heads)
    upto = jnp.tril(jnp.ones((BLOCK, BLOCK), jnp.float32))
    cumulative = jnp.einsum(
        "js,csh->cjh", upto, logs.reshape(blocks, BLOCK, heads), precision=HIGHEST
    )
    last = cumulative[:, -1]
    weight_logs = last[:, None, :] - cumulative + inputs
    peak = jnp.max(weight_logs, axis=1)
    coefficients = jnp.exp(weight_logs - peak[:, None, :])
    scaled = keys.reshape(blocks, BLOCK, heads, DK).astype(jnp.float32) * DK ** (-0.5)
    weighted_keys = scaled * coefficients[..., None]
    value_float = values.reshape(blocks, BLOCK, heads, DV).astype(jnp.float32)
    states = jnp.einsum("cshk,cshv->chkv", weighted_keys, value_float, precision=HIGHEST)
    place = jnp.arange(blocks)
    between = (place[None, :, None] < place[None, None, :]) & (
        place[None, None, :] < place[:, None, None]
    )
    decay = jnp.sum(jnp.where(between[..., None], last[None, None], 0.0), axis=2) + peak[None]
    earlier = (place[None, :] < place[:, None])[..., None]
    decay = jnp.where(earlier, decay, -jnp.inf)
    start = jnp.sum(jnp.where(earlier, last[None], 0.0), axis=1)
    ceiling = jnp.maximum(start, jnp.max(decay, axis=1))
    shares = jnp.exp(decay - ceiling[:, None])
    before = jnp.einsum("cdh,dhkv->chkv", shares, states, precision=HIGHEST)
    return ((before, ceiling), cumulative, inputs)


def spread_kernel(first, second, n, m, x_ref, out_ref, local_sem, send, recv, send_on, recv_on):
    me = lax.axis_index(first)
    mine = lax.axis_index(second)
    barrier = pltpu.get_barrier_semaphore()
    mesh_ids = pl.DeviceIdType.MESH
    for k in range(1, n):
        pl.semaphore_signal(
            barrier, inc=1, device_id={first: lax.rem(me + k, n)}, device_id_type=mesh_ids
        )
    for k in range(1, m):
        pl.semaphore_signal(
            barrier, inc=1, device_id={second: lax.rem(mine + k, m)}, device_id_type=mesh_ids
        )
    pl.semaphore_wait(barrier, n + m - 2)
    copies = []
    for k in range(1, n):
        peer = lax.rem(me + k, n)
        copy = pltpu.make_async_remote_copy(
            src_ref=x_ref.at[peer],
            dst_ref=out_ref.at[me, mine],
            send_sem=send.at[k - 1],
            recv_sem=recv.at[k - 1],
            device_id={first: peer},
            device_id_type=mesh_ids,
        )
        copy.start()
        copies.append(copy)
    kept = pltpu.make_async_copy(x_ref.at[me], out_ref.at[me, mine], local_sem)
    kept.start()
    onward = []
    for k in range(n):
        source = lax.rem(me - k + n, n)
        if k > 0:
            copies[k - 1].wait_recv()
        block = x_ref.at[me] if k == 0 else out_ref.at[source, mine]
        for j in range(1, m):
            copy = pltpu.make_async_remote_copy(
                src_ref=block,
                dst_ref=out_ref.at[source, mine],
                send_sem=send_on.at[k, j - 1],
                recv_sem=recv_on.at[k, j - 1],
                device_id={second: lax.rem(mine + j, m)},
                device_id_type=mesh_ids,
            )
            copy.start()
            onward.append(copy)
    kept.wait()
    for copy in copies:
        copy.wait_send()
    for k in range(n):
        for j in range(1, m):
            copy = onward[k * (m - 1) + j - 1]
            copy.wait_send()
            copy.wait_recv()


def spread(x, first, second, number):
    n, m = lax.axis_size(first), lax.axis_size(second)
    shape = (n, m) + x.shape[1:]
    size = x.size * x.dtype.itemsize * m
    return pl.pallas_call(
        lambda *refs: spread_kernel(first, second, n, m, *refs),
        out_shape=jax.ShapeDtypeStruct(shape, x.dtype),
        in_specs=[pl.BlockSpec(memory_space=pltpu.VMEM)],
        out_specs=pl.BlockSpec(memory_space=pltpu.VMEM),
        scratch_shapes=[
            pltpu.SemaphoreType.DMA,
            pltpu.SemaphoreType.DMA((n - 1,)),
            pltpu.SemaphoreType.DMA((n - 1,)),
            pltpu.SemaphoreType.DMA((n, m - 1)),
            pltpu.SemaphoreType.DMA((n, m - 1)),
        ],
        compiler_params=pltpu.CompilerParams(collective_id=number, has_side_effects=True),
        cost_estimate=pl.CostEstimate(flops=0, bytes_accessed=30 * size, transcendentals=0),
    )(x)


def both_halves(own, axis):
    if lax.axis_size("tp") != 2:
        return lax.all_gather(own, "tp", axis=axis, tiled=True)
    other = lax.ppermute(own, "tp", [(0, 1), (1, 0)])
    first = lax.axis_index("tp") == 0
    return jnp.concatenate(
        [jnp.where(first, own, other), jnp.where(first, other, own)], axis=axis
    )


def resharded(
    tokens,
    norm_gain,
    query_weight,
    key_weight,
    value_weight,
    outgate_weight,
    gate_weight,
    forget_bias,
    forget_shift,
    head_norm_gain,
    exit_weight,
    entry_weight,
    signal_weight,
    conv_kernel,
    merge_weight,
):
    parts = lax.axis_size("sp")
    place = lax.axis_index("sp")
    depth = key_weight.shape[0]
    gates = gate_weight.shape[2]
    heads = gates // parts
    stack = [
        query_weight,
        key_weight,
        value_weight,
        outgate_weight,
        exit_weight,
        entry_weight,
        signal_weight,
        gate_weight.reshape(depth, 2, parts, heads).swapaxes(1, 2).reshape(depth, -1),
    ]
    widths = [w.size // depth // parts for w in stack]
    spare = jnp.zeros((depth, -sum(widths) % 128), jnp.bfloat16)
    stacked = jnp.stack(
        [
            jnp.concatenate(
                [w[:, p * width : (p + 1) * width] for w, width in zip(stack, widths)] + [spare],
                axis=1,
            )
            for p in range(parts)
        ]
    )
    rows = spread(stacked, "sp", "fs", 0)
    rows = rows.reshape(-1, rows.shape[-1])
    line = lax.all_gather(tokens[0], "sp", axis=0, tiled=True)
    rows, line, merge_weight = lax.optimization_barrier((rows, line, merge_weight))
    whole = both_halves(line, 1)
    count = whole.shape[0]
    flat = whole.astype(jnp.float32)
    normed = (
        flat * lax.rsqrt(jnp.mean(flat * flat, axis=-1, keepdims=True) + EPSILON) * norm_gain
    ).astype(jnp.bfloat16)
    total = add_product(normed, rows)
    columns = []
    offset = 0
    for width in widths:
        columns.append(total[:, offset : offset + width])
        offset = offset + width
    queries, keys, values, outgates, exit_rows, entry_rows, signal_rows = [
        c.astype(jnp.bfloat16) for c in columns[:7]
    ]
    gate_pre = columns[7]

    def own(array, axis, width):
        return lax.dynamic_slice_in_dim(array, place * width, width, axis)

    shift = lax.all_to_all(forget_shift[0].reshape(parts, heads, -1), "sp", 0, 0)
    shift = shift.transpose(1, 0, 2).reshape(heads, count)
    logs = jax.nn.log_sigmoid(gate_pre[:, heads:] + own(forget_bias, 0, heads)) + shift.T
    blocks = count // BLOCK
    apertures, cumulative, inputs = whole_states(keys, values, gate_pre[:, :heads], logs, blocks)
    channels = exit_rows.shape[1]
    taps = own(conv_kernel, 1, channels)
    mixed_in = (entry_rows.astype(jnp.float32) * signal_rows.astype(jnp.float32)).astype(
        jnp.bfloat16
    )
    padded = jnp.pad(mixed_in, ((KERNEL - 1, 0), (0, 0))).astype(jnp.float32)
    response = taps[0] * padded[0:count]
    for tap in range(1, KERNEL):
        response = response + taps[tap] * padded[tap : tap + count]
    conv_out = (exit_rows.astype(jnp.float32) * response).astype(jnp.bfloat16)
    memory_out = memory_output(
        queries,
        keys,
        values,
        outgates,
        inputs,
        cumulative,
        apertures,
        own(head_norm_gain, 0, heads * DV),
    )
    both = jnp.concatenate([memory_out, conv_out], axis=1)
    halves = spread(both.reshape(parts, count // parts, -1), "sp", "tp", 1)
    memory_width = heads * DV
    pieces = [(t, p) for t in range(halves.shape[1]) for p in range(parts)]
    merged_in = jnp.concatenate(
        [halves[p, t, :, :memory_width] for t, p in pieces]
        + [halves[p, t, :, memory_width:] for t, p in pieces],
        axis=1,
    )
    merge = lax.all_gather(merge_weight, ("sp", "fs"), axis=0, tiled=True)
    mixed = add_product(merged_in, merge)
    return mixed.astype(jnp.bfloat16)[None]


def solution(mesh):
    placed = (
        P("fs", "sp", "tp"),
        P(),
        P(("sp", "fs"), "tp"),
        P(("sp", "fs"), "tp"),
        P(("sp", "fs"), "tp"),
        P(("sp", "fs"), "tp"),
        P(("sp", "fs"), None, "tp"),
        P("tp"),
        P("fs", "tp", "sp"),
        P("tp"),
        P(("sp", "fs"), "tp"),
        P(("sp", "fs"), "tp"),
        P(("sp", "fs"), "tp"),
        P(None, "tp"),
        P(("sp", "fs"), "tp"),
    )
    sp, tp = mesh.shape["sp"], mesh.shape["tp"]

    def step(*args):
        heads, channels = args[6].shape[2], args[10].shape[1]
        many = min(sp, mesh.shape["fs"], tp) > 1
        even = heads % (sp * tp) == 0 and channels % (sp * tp * 128) == 0
        body = resharded if many and even else local
        return jax.shard_map(
            body, mesh=mesh, in_specs=placed, out_specs=P("fs", "sp", "tp"), check_vma=False
        )(*args)

    return step
```

profile of v0, /device:TPU:9, one launch (start us, length us, event | category | flops | bytes accessed | tf_op | source)
XLA Modules:
  0.0 345.6 jit_solution(6777703396418532237)
XLA Ops:
  13.1 1.5 pad_maximum_fusion.3.refs_0_
  14.6 103.1 %shard_map.145 = bf16[4,4,128,1664]{3,2,1,0:T(8,128)(2,1)} custom-call(bf16[4,128,1664]{2,1,0:T(8,128)(2,1)} %pad_maximum_fusion.3.refs_0_), custom_call_target="tpu_custom_call" | custom-call | bytes 204472320 | tf_op jit(solution)/shard_map/pallas_call | solution.py:294
  117.7 5.2 %all-gather.6.cloned.1.call-done = bf16[1,2048,1024]{2,1,0:T(8,128)(2,1)} async-done(((bf16[1,512,1024]{2,1,0:T(8,128)(2,1)}), bf16[1,2048,1024]{2,1,0:T(8,128)(2,1)}) %all-gather.6.cloned.1.call-update) | async-done | bytes 4194320 | tf_op jit(solution)/shard_map/all_gather | solution.py:366
  124.0 23.6 %all-to-all-start = ((f32[4,2,512]{2,1,0:T(2,128)}), f32[4,2,512]{2,1,0:T(2,128)S(1)}, u32[]{:S(2)}, u32[]{:S(2)}) async-start(f32[4,2,512]{2,1,0:T(2,128)} %reshape_squeeze.3), calls=%async_computation | async-start | bytes 32768 | tf_op jit(solution)/shard_map/all_to_all | solution.py:388
  149.4 3.9 %broadcast_select_fusion.1 = (bf16[2048,1024]{1,0:T(8,128)(2,1)S(1)}, bf16[2048,1024]{1,0:T(8,128)(2,1)S(1)}) fusion(bf16[2048,1024]{1,0:T(8,128)(2,1)} %bitcast.138, bf16[2048,1024]{1,0:T(8,128)(2,1)} %collective-permute-done, pred[]{:T(512)S(6)} %eq.3), kind=kLoop, calls=%fused_computation.10 | loop fusion | flops 4194304 | bytes 16777216 | tf_op jit(solution)/shard_map/jit(_where)/select_n | solution.py:317
  153.3 1.9 fusion
  156.6 23.1 %fusion.75 = (bf16[2048,1664]{0,1:T(8,128)(2,1)}, f32[2048,1664]{0,1:T(8,128)}) fusion(bf16[2048,1664]{1,0:T(8,128)(2,1)} %bitcast.136, f32[2048]{0:T(1024)S(1)} %copy-done.5, f32[2048]{0:T(1024)S(1)} %add_rsqrt_fusion, bf16[2048,1024]{1,0:T(8,128)(2,1)} %copy-done.1, bf16[2048,1024]{1,0:T(8,128)(2,1)} %copy-done), kind=kOutput, calls=%fused_computation.129 | convolution fusion | flops 13991411712 | bytes 35667968 | tf_op jit(solution)/shard_map/dot_general | solution.py:55
  188.6 1.6 convolution_bitcast_fusion
  190.3 1.9 fusion.18
  192.2 4.6 %multiply_reduce_fusion = (f32[16,2,128]{2,1,0:T(2,128)S(1)}, f32[16,2,128,128]{2,3,1,0:T(8,128)}) fusion(f32[16,2,128,128]{2,3,1,0:T(8,128)S(1)} %fusion.18, f32[16,2,128]{2,1,0:T(2,128)S(1)} %copy.157, bf16[16,128,2,128]{3,1,2,0:T(8,128)(2,1)S(1)} %copy.152, f32[16,2,128]{2,1,0:T(2,128)S(1)} %copy.145, f32[16,2,128]{2,1,0:T(2,128)S(1)} %copy.139, ...), kind=kOutput, calls=%fused_computation.26 | convolution fusion | flops 207089664 | bytes 6389760 | tf_op jit(solution)/shard_map/chjs,cshv->chjv/dot_general | solution.py:124
  196.8 2.1 fusion.14
  200.2 3.3 fusion.8
  203.8 2.7 fusion.11
  207.0 2.5 copy.159
  209.5 91.9 %shard_map.146 = bf16[4,2,512,512]{3,2,1,0:T(8,128)(2,1)} custom-call(bf16[4,512,512]{2,1,0:T(8,128)(2,1)} %bitcast.134), custom_call_target="tpu_custom_call" | custom-call | bytes 125829120 | tf_op jit(solution)/shard_map/pallas_call | solution.py:294
  301.4 1.7 bitcast_dynamic-update-slice_fusion.15
  303.1 1.7 bitcast_dynamic-update-slice_fusion.14
  304.8 1.7 bitcast_dynamic-update-slice_fusion.13
  306.5 1.7 bitcast_dynamic-update-slice_fusion.12
  308.2 1.7 bitcast_dynamic-update-slice_fusion.11
  309.9 1.7 bitcast_dynamic-update-slice_fusion.10
  311.6 1.7 bitcast_dynamic-update-slice_fusion.9
  313.3 1.7 bitcast_dynamic-update-slice_fusion.8
  315.0 1.7 bitcast_dynamic-update-slice_fusion.7
  316.7 1.7 bitcast_dynamic-update-slice_fusion.6
  318.4 1.7 bitcast_dynamic-update-slice_fusion.5
  320.1 1.7 bitcast_dynamic-update-slice_fusion.4
  321.8 1.7 bitcast_dynamic-update-slice_fusion.3
  323.5 1.7 bitcast_dynamic-update-slice_fusion.2
  325.2 1.7 bitcast_dynamic-update-slice_fusion.1
  326.9 1.7 bitcast_dynamic-update-slice_fusion
  328.7 10.1 %fusion.17 = bf16[1,512,1024]{2,1,0:T(8,128)(2,1)} fusion(bf16[512,4096]{1,0:T(8,128)(2,1)} %bitcast_dynamic-update-slice_fusion, bf16[4096,1024]{1,0:T(8,128)(2,1)} %all-gather.4.cloned.1.call-done), kind=kOutput, calls=%fused_computation.33 | convolution fusion | flops 4295491584 | bytes 13631488 | tf_op jit(solution)/shard_map/dot_general | solution.py:55
  (76 shorter events, 21.5 us)
Async XLA Ops:
  6.5 116.4 %all-gather.6.cloned.1.call-start = ((), (), s32[]{:S(2)}) async-start(), calls=%async_computation.2 | async-start | bytes 5242880 | tf_op jit(solution)/shard_map/all_gather | solution.py:366
  7.3 321.4 %all-gather.4.cloned.1.call-start = ((), (), s32[]{:S(2)}) async-start(), calls=%async_computation.1 | async-start | bytes 8912896 | tf_op jit(solution)/shard_map/all_gather | solution.py:422
  14.6 108.8 %copy-start.4 = (f32[1,8,512]{2,1,0:T(8,128)S(1)}, f32[1,8,512]{2,1,0:T(8,128)}, u32[]{:S(2)}) copy-start(f32[1,8,512]{2,1,0:T(8,128)} %param.23) | copy-start | bytes 49156
  14.6 133.0 %copy-start.6 = (f32[8]{0:T(128)S(1)}, f32[8]{0:T(128)}, u32[]{:S(2)}) copy-start(f32[8]{0:T(128)} %param.22) | copy-start | bytes 100
  122.9 26.4 %collective-permute-start = (bf16[2048,1024]{1,0:T(8,128)(2,1)}, bf16[2048,1024]{1,0:T(8,128)(2,1)}, u32[]{:S(2)}, u32[]{:S(2)}) collective-permute-start(bf16[2048,1024]{1,0:T(8,128)(2,1)} %bitcast.137), channel_id=1, source_target_pairs={{0,1},{1,0},{2,3},{3,2},{4,5},{5,4},{6,7},{7,6},{8,9},{9,8},{10,11... | collective-permute-start | bytes 12582920 | tf_op jit(solution)/shard_map/ppermute | solution.py:314
  124.0 55.7 %all-to-all-start = ((f32[4,2,512]{2,1,0:T(2,128)}), f32[4,2,512]{2,1,0:T(2,128)S(1)}, u32[]{:S(2)}, u32[]{:S(2)}) async-start(f32[4,2,512]{2,1,0:T(2,128)} %reshape_squeeze.3), calls=%async_computation | async-start | bytes 32768 | tf_op jit(solution)/shard_map/all_to_all | solution.py:388
  153.3 2.0 copy-start
  153.3 3.3 copy-start.1
  153.3 3.3 copy-start.5
  187.5 2.8 copy-start.2
  187.6 2.6 copy-start.3
Sparse Core Ops, SparseCore 0:
  8.9 113.9 all-gather.5
  125.7 165.7 all-gather.3
where the time goes:
time: 347 us; the launch traced here: 346 us
  Pallas kernels  195 us (56%)
  local copies, waits for them, and re-layouts  45.1 us (13%)
  matrix products  42.5 us (12%)
  starting transfers between devices  24 us (7%)
  other arithmetic  19.2 us (6%)
  between operations  13.8 us (4%)
  waiting for transfers between devices  5.93 us (2%)
    pallas_call x2, Pallas kernels, spread(): pl.pallas_call(lambda *refs: spread_kernel(first, second, n, m, *refs), o...  195 us
    dot_general x2, matrix products, add_product(): return jnp.dot(left, piece, preferred_element_type=jnp.float32)  33.2 us
    unnamed x41, local copies, waits for them, and re-layouts  30.7 us
    all_to_all x1, starting transfers between devices, resharded(): lax.all_to_all(forget_shift[0].reshape(parts, heads, -1), 'sp', 0, 0)  23.6 us
  transfers between devices with their start and end apart: 4, of which 1 were waited for; matrix products, arithmetic and copies ran while one was open for 28% of the time, Pallas kernels for 56%

commit v1 on v0

v1 whole, which is shorter than its diff:
```python
import jax
import jax.numpy as jnp
from jax import lax
from jax.experimental import pallas as pl
from jax.experimental.pallas import tpu as pltpu
from jax.sharding import PartitionSpec as P

DK = 64
DV = 128
BLOCK = 128
KERNEL = 3


EPSILON = 1e-06
EMPTY_LOG = -1e30
HIGHEST = lax.Precision.HIGHEST


def prefix(part, axis, combine, identity):
    place = lax.axis_index(axis)
    gathered = jax.tree.map(lambda a: lax.all_gather(a, axis), part)
    state = jax.tree.map(lambda a, e: jnp.zeros_like(a) + jnp.asarray(e, a.dtype), part, identity)

    def one(step, state):
        return combine(
            state, jax.tree.map(lambda a: lax.dynamic_index_in_dim(a, step, 0, False), gathered)
        )

    return lax.fori_loop(0, place, one, state)


def passed_along(value, axis, steps):
    count = lax.axis_size(axis)
    initial, last = (max(0, -steps), min(count, count - steps))
    return lax.ppermute(value, axis, [(source, source + steps) for source in range(initial, last)])


def combine(earlier, later):
    ceiling = jnp.maximum(later[2] + earlier[1], later[1])
    kept = jnp.exp(later[2] + earlier[1] - ceiling)
    added = jnp.exp(later[1] - ceiling)
    state = kept[..., None, None] * earlier[0] + added[..., None, None] * later[0]
    return (state, ceiling, earlier[2] + later[2])


def identity_state(heads):
    return (
        jnp.zeros((heads, DK, DV), jnp.float32),
        jnp.full((heads,), EMPTY_LOG, jnp.float32),
        jnp.zeros((heads,), jnp.float32),
    )


def add_product(left, piece):
    return jnp.dot(left, piece, preferred_element_type=jnp.float32)


def split_columns(total, stack):
    outputs = []
    offset = 0
    for weight in stack:
        outputs.append(total[:, offset : offset + weight.shape[1]])
        offset = offset + weight.shape[1]
    return outputs


def incoming_state(running):
    heads = running[1].shape[0]
    before = prefix((running[0], running[1], running[2]), "sp", combine, identity_state(heads))
    ceiling = jnp.maximum(before[1], before[2])
    shrink = jnp.exp(before[1] - ceiling)
    return (before[0] * shrink[:, None, None], ceiling, before[2])


def memory_states(keys, values, gates, forget_bias, forget_shift):
    count = gates.shape[0]
    heads = forget_bias.shape[0]
    blocks = count // BLOCK
    inputs = gates[:, :heads].reshape(blocks, BLOCK, heads)
    logs = jax.nn.log_sigmoid(gates[:, heads:] + forget_bias) + forget_shift[0].T
    cumulative = jnp.cumsum(logs.reshape(blocks, BLOCK, heads), axis=1)
    last = cumulative[:, -1]
    weight_logs = last[:, None, :] - cumulative + inputs
    peak = jnp.max(weight_logs, axis=1)
    coefficient_array = jnp.exp(weight_logs - peak[:, None, :])
    scaled = keys.reshape(blocks, BLOCK, heads, DK).astype(jnp.float32) * DK ** (-0.5)
    value_float = values.reshape(blocks, BLOCK, heads, DV).astype(jnp.float32)
    states = jnp.einsum(
        "csh,cshk,cshv->chkv", coefficient_array, scaled, value_float, precision=HIGHEST
    )
    running = identity_state(heads)
    prefixes = []
    for index in range(blocks):
        prefixes.append(running)
        running = combine(running, (states[index], peak[index], last[index]))
    leading_part = tuple((jnp.stack([item[member] for item in prefixes]) for member in range(3)))
    gate_apertures = combine(incoming_state(running), leading_part)
    return (gate_apertures, cumulative, inputs)


def memory_output(
    queries, keys, values, outgates, inputs, cumulative, gate_apertures, head_norm_gain
):
    blocks = cumulative.shape[0]
    heads = cumulative.shape[2]
    count = queries.shape[0]
    query_blocks = queries.reshape(blocks, BLOCK, heads, DK)
    key_blocks = keys.reshape(blocks, BLOCK, heads, DK)
    value_blocks = values.reshape(blocks, BLOCK, heads, DV)
    score_matrix = jnp.einsum(
        "cjhk,cshk->chjs", query_blocks, key_blocks, preferred_element_type=jnp.float32
    ) * DK ** (-0.5)
    cum_lanes = cumulative.transpose(0, 2, 1)
    input_lanes = inputs.transpose(0, 2, 1)
    causal = jnp.tril(jnp.ones((BLOCK, BLOCK), dtype=bool))
    decay = jnp.where(
        causal,
        cum_lanes[..., :, None] - cum_lanes[..., None, :] + input_lanes[..., None, :],
        -jnp.inf,
    )
    inter = cum_lanes + gate_apertures[1][..., None]
    ceiling = jnp.maximum(inter, jnp.max(decay, axis=-1))
    weighted = score_matrix * jnp.exp(decay - ceiling[..., None])
    numerator = jnp.einsum(
        "chjs,cshv->chjv",
        weighted.astype(jnp.bfloat16),
        value_blocks,
        preferred_element_type=jnp.float32,
    )
    query_float = query_blocks.astype(jnp.float32)
    carried = jnp.exp(inter - ceiling)
    numerator = numerator + carried[..., None] * jnp.einsum(
        "cjhk,chkv->chjv", query_float, gate_apertures[0], precision=HIGHEST
    )
    result = numerator * lax.rsqrt(
        jnp.mean(numerator * numerator, axis=-1, keepdims=True) + EPSILON
    )
    result = result.transpose(0, 2, 1, 3).reshape(count, heads * DV) * head_norm_gain
    return (result * jax.nn.sigmoid(outgates.astype(jnp.float32))).astype(jnp.bfloat16)


def local(
    tokens,
    norm_gain,
    query_weight,
    key_weight,
    value_weight,
    outgate_weight,
    gate_weight,
    forget_bias,
    forget_shift,
    head_norm_gain,
    exit_weight,
    entry_weight,
    signal_weight,
    conv_kernel,
    merge_weight,
):
    whole = lax.all_gather(tokens, "tp", axis=2, tiled=True)[0]
    count = whole.shape[0]
    flat = whole.astype(jnp.float32)
    normed = (
        flat * lax.rsqrt(jnp.mean(flat * flat, axis=-1, keepdims=True) + EPSILON) * norm_gain
    ).astype(jnp.bfloat16)
    gate_rows = gate_weight.reshape(gate_weight.shape[0], -1)
    state_stack = [key_weight, value_weight, gate_rows]
    other_stack = [query_weight, outgate_weight, exit_weight, entry_weight, signal_weight]
    stacked = jnp.concatenate(state_stack + other_stack, axis=1)
    total = add_product(normed, lax.all_gather(stacked, ("sp", "fs"), axis=0, tiled=True))
    columns = split_columns(total, state_stack + other_stack)
    keys = columns[0].astype(jnp.bfloat16)
    values = columns[1].astype(jnp.bfloat16)
    gate_apertures, cumulative, inputs = memory_states(
        keys, values, columns[2], forget_bias, forget_shift
    )
    others = columns[3:]
    queries = others[0].astype(jnp.bfloat16)
    outgates = others[1].astype(jnp.bfloat16)
    exit_rows = others[2].astype(jnp.bfloat16)
    entry_rows = others[3].astype(jnp.bfloat16)
    signal_rows = others[4].astype(jnp.bfloat16)
    mixed_in = (entry_rows.astype(jnp.float32) * signal_rows.astype(jnp.float32)).astype(
        jnp.bfloat16
    )
    rim = passed_along(mixed_in[count - (KERNEL - 1) :], "sp", 1)
    padded = jnp.concatenate([rim, mixed_in], axis=0).astype(jnp.float32)
    response = conv_kernel[0] * padded[0:count]
    for tap in range(1, KERNEL):
        response = response + conv_kernel[tap] * padded[tap : tap + count]
    conv_out = (exit_rows.astype(jnp.float32) * response).astype(jnp.bfloat16)
    memory_out = memory_output(
        queries, keys, values, outgates, inputs, cumulative, gate_apertures, head_norm_gain
    )
    memory_all, conv_all = (
        lax.all_gather(memory_out, "tp", axis=1, tiled=True),
        lax.all_gather(conv_out, "tp", axis=1, tiled=True),
    )
    concatenated_result = jnp.concatenate([memory_all, conv_all], axis=1)
    mixed = add_product(
        concatenated_result, lax.all_gather(merge_weight, ("sp", "fs"), axis=0, tiled=True)
    )
    return mixed.astype(jnp.bfloat16)[None]


MESH = pl.DeviceIdType.MESH


class Place:
    def __init__(self):
        self.z = lax.axis_index("sp")
        f = lax.axis_index("fs")
        self.t = lax.axis_index("tp")
        self.h, self.p = self.z // 2, self.z % 2
        self.y, self.x = f // 2, f % 2
        self.c = self.p * 2 + self.x
        self.xn = {"fs": self.y * 2 + 1 - self.x}
        self.yn = {"fs": (1 - self.y) * 2 + self.x}
        self.tn = {"tp": 1 - self.t}
        self.row = [
            self.z,
            self.h * 2 + 1 - self.p,
            (1 - self.h) * 2 + self.p,
            (1 - self.h) * 2 + 1 - self.p,
        ]
        self.zn = [None] + [{"sp": row} for row in self.row[1:]]
        self.diagonal = {"fs": self.y * 2 + 1 - self.x, "sp": self.row[1]}
        self.block = {
            (i, j): (self.x + i - 2 * i * self.x) * 2 + (self.p + j - 2 * j * self.p)
            for i in range(2)
            for j in range(2)
        }

    def greet(self, peers):
        barrier = pltpu.get_barrier_semaphore()
        for peer in peers:
            pl.semaphore_signal(barrier, inc=1, device_id=peer, device_id_type=MESH)
        pl.semaphore_wait(barrier, len(peers))


class Sender:
    def __init__(self, send_sem, recv_sem):
        self.send_sem, self.recv_sem, self.copies = send_sem, recv_sem, {}

    def make(self, name, source, target, peer):
        index = len(self.copies)
        self.copies[name] = pltpu.make_async_remote_copy(
            src_ref=source,
            dst_ref=target,
            send_sem=self.send_sem.at[index],
            recv_sem=self.recv_sem.at[index],
            device_id=peer,
            device_id_type=MESH,
        )
        return self.copies[name]

    def __call__(self, name, source, target, peer):
        self.make(name, source, target, peer).start()

    def arrived(self, name):
        self.copies[name].wait_recv()

    def drain(self):
        for copy in self.copies.values():
            copy.wait_send()


MERGE_SLICES = 2


def layer_kernel(heads, groups, *refs):
    widths = sum(groups, [])
    count = len(widths)
    gain_ref, tokens_ref, shift_ref, gate_ref, bias_ref, head_gain_ref, taps_ref, merge_ref = refs[:8]
    weights = refs[8 : 8 + count]
    out_ref = refs[8 + count]
    (
        tok,
        normed,
        stage,
        transit,
        rows_ref,
        gate_rows,
        shifts_ref,
        proj,
        parts,
        pieces,
        both,
        entered,
        held,
        keys_t,
        u_ref,
        top_ref,
        last_ref,
        states,
        stable,
        decayed,
        final_state,
        final_log,
        came_state,
        came_log,
        rim,
        came_rim,
        own_sum,
        partial,
        came,
        relayed,
        local,
        send_sem,
        recv_sem,
    ) = refs[9 + count :]
    at = Place()
    z, y, x, t, p, c = at.z, at.y, at.x, at.t, at.p, at.c
    mine, by_z, by_x, by_both = (at.block[i] for i in ((0, 0), (0, 1), (1, 0), (1, 1)))
    depth = weights[0].shape[0]
    half_rows = parts.shape[1]
    broad = rows_ref.shape[2]
    tokens = tok.shape[2]
    features = normed.shape[1]
    width_t = features // 2
    per = tokens // BLOCK
    blocks = 2 * per
    other_x, other_p = 1 - x, 1 - p
    kept = []

    def fetch(source, target):
        copy = pltpu.make_async_copy(source, target, local.at[len(kept)])
        copy.start()
        kept.append(copy)

    def rows_of(k, beside, side):
        row = at.row[k] * 4 + (1 - y if beside else y) * 2 + (other_x if side else x)
        return pl.ds(pl.multiple_of(row * depth, depth), depth)

    def slab(k, side, s):
        return rows_ref.at[s, rows_of(k, False, side)]

    def lanes(k, side):
        return gate_rows.at[:, rows_of(k, False, side)]

    fetch(tokens_ref, tok.at[mine, t])
    fetch(shift_ref, shifts_ref.at[mine])
    fetch(gate_ref, lanes(0, 0))
    fetch(merge_ref.at[pl.ds(0, half_rows)], parts.at[y])
    for quarter in range(4):
        index = 0
        for s, group in enumerate(groups):
            offset = 0
            for width in group:
                fetch(
                    weights[index].at[:, pl.ds(quarter * width, width)],
                    stage.at[quarter, s, :, pl.ds(offset, width)],
                )
                offset += width
                index += 1
    at.greet([at.xn, at.yn, at.tn, at.diagonal] + at.zn[1:])
    for copy in kept:
        copy.wait()

    send = Sender(send_sem, recv_sem)

    def to_z(side, s):
        for k in (1, 3, 2):
            if side:
                source = slab(0, 1, s) if k == 2 else transit.at[s]
            else:
                source = stage.at[(p if k == 2 else other_p) * 2 + x, s]
            send(("z", k, side, s), source, slab(0, side, s), at.zn[k])

    for k in (1, 2, 3):
        send(("zg", k, 0), lanes(0, 0), lanes(0, 0), at.zn[k])
    send("x gate", lanes(0, 0), lanes(0, 0), at.xn)
    send(("yg", 0, 0), lanes(0, 0), lanes(0, 0), at.yn)
    send("x shift", shifts_ref.at[mine], shifts_ref.at[mine], at.xn)
    send("z shift", shifts_ref.at[mine], shifts_ref.at[mine], at.zn[1])

    def to_x(s):
        send(("x same", s), stage.at[p * 2 + other_x, s], slab(0, 0, s), at.xn)
        send(("x other", s), stage.at[other_p * 2 + other_x, s], transit.at[s], at.xn)

    def to_y(side, s):
        source = slab(0, 1, s) if side else stage.at[c, s]
        send(("y", 0, side, s), source, slab(0, side, s), at.yn)

    to_x(0)
    to_z(0, 0)
    to_y(0, 0)
    send("t own", tok.at[mine, t], tok.at[mine, t], at.tn)
    send("z tok", tok.at[mine, t], tok.at[mine, t], at.zn[1])
    send("part", merge_ref.at[pl.ds(half_rows, half_rows)], parts.at[y], at.yn)
    for s in range(len(groups)):
        rows_ref[s, rows_of(0, False, 0), :] = stage[c, s]

    gain = gain_ref[...]
    step = 16

    def normalize(block):
        def one(i, carry):
            local_rows = pl.ds(pl.multiple_of(i * step, step), step)
            halves = [tok[block, side, local_rows, :].astype(jnp.float32) for side in range(2)]
            total = sum(jnp.sum(a * a, axis=1, keepdims=True) for a in halves)
            scale = lax.rsqrt(total / features + EPSILON)
            place = pl.ds(pl.multiple_of(block * tokens + i * step, step), step)
            for side in range(2):
                columns = slice(side * width_t, (side + 1) * width_t)
                value = halves[side] * scale * gain[:, columns]
                normed[place, columns] = value.astype(jnp.bfloat16)
            return carry

        lax.fori_loop(0, tokens // step, one, 0, unroll=4)

    def project(block, s):
        place = pl.ds(pl.multiple_of(block * tokens, tokens), tokens)

        def one(n, carry):
            columns = pl.ds(pl.multiple_of(n * 512, 512), 512)
            product = jnp.dot(
                normed[place, :], rows_ref[s, :, columns], preferred_element_type=jnp.float32
            )
            proj[s, place, columns] = product.astype(jnp.bfloat16)
            return carry

        lax.fori_loop(0, broad // 512, one, 0)

    def forward(side, s):
        for k in (1, 3, 2):
            if s == 0:
                send.arrived(("zg", k, side))
                send(("yg", k, side), lanes(k, side), lanes(k, side), at.yn)
            send.arrived(("z", k, side, s))
            send(("y", k, side, s), slab(k, side, s), slab(k, side, s), at.yn)

    def all_here(s):
        for k in range(4):
            for side in range(2):
                send.arrived(("y", k, side, s))

    half_at = (y + p - 2 * y * p) * half_rows
    out_strip = pieces.shape[2] // MERGE_SLICES

    def merge_half(k, parity, s):
        side = y + parity - 2 * y * parity
        place = pl.ds(pl.multiple_of(side * half_rows, half_rows), half_rows)
        return pieces.at[at.row[k], place, pl.ds(s * out_strip, out_strip)]

    def merge_to_z(s):
        for k in (1, 3, 2):
            source = parts.at[p if k == 2 else other_p, :, pl.ds(s * out_strip, out_strip)]
            parity = p if k == 2 else other_p
            send(("m", k, s), source, merge_half(0, parity, s), at.zn[k])

    def merge_to_y(s):
        source = parts.at[p, :, pl.ds(s * out_strip, out_strip)]
        send(("my", 0, s), source, merge_half(0, p, s), at.yn)

    def forward_merge(s):
        for k in (1, 3, 2):
            send.arrived(("m", k, s))
            send(("my", k, s), merge_half(k, p, s), merge_half(k, p, s), at.yn)

    send.arrived("t own")
    normalize(mine)
    send.arrived(("x same", 0))
    to_y(1, 0)
    send.arrived("x gate")
    send(("yg", 0, 1), lanes(0, 1), lanes(0, 1), at.yn)
    for k in (1, 2, 3):
        send(("zg", k, 1), lanes(0, 1), lanes(0, 1), at.zn[k])
    send.arrived(("x other", 0))
    to_z(1, 0)
    send("x tok", tok.at[mine, t], tok.at[mine, t], at.xn)
    to_x(1)
    to_z(0, 1)
    forward(0, 0)
    to_z(0, 2)
    to_y(0, 1)
    send.arrived("part")
    pieces[z, pl.ds(pl.multiple_of(half_at, half_rows), half_rows), :] = parts[p]
    forward(1, 0)
    to_y(0, 2)
    send.arrived("z tok")
    send("t z", tok.at[by_z, t], tok.at[by_z, t], at.tn)
    send.arrived("z shift")
    send.arrived("x tok")
    send("t x", tok.at[by_x, t], tok.at[by_x, t], at.tn)
    to_x(2)
    send("x tok on", tok.at[by_z, t], tok.at[by_z, t], at.xn)
    send("x shift on", shifts_ref.at[by_z], shifts_ref.at[by_z], at.xn)
    send.arrived(("x same", 1))
    to_y(1, 1)
    send.arrived(("x other", 1))
    to_z(1, 1)
    send.arrived("t z")
    normalize(by_z)
    forward(0, 1)
    send.arrived("t x")
    normalize(by_x)
    for k in range(4):
        for side in range(2):
            send.arrived(("yg", k, side))
    all_here(0)

    kq, kv = heads * DK, heads * DV
    q_at, k_at, v_at = 0, groups[0][0], groups[0][0] + groups[0][1]
    conv = groups[1][0]
    scale = DK ** (-0.5)
    lane = lax.broadcasted_iota(jnp.int32, (BLOCK, BLOCK), 1)
    sub = lax.broadcasted_iota(jnp.int32, (BLOCK, BLOCK), 0)
    causal = lane <= sub
    upto = (sub <= lane).astype(jnp.float32)
    which = lax.broadcasted_iota(jnp.int32, shifts_ref.shape[1:], 0)
    tp_heads = gate_rows.shape[0] // 2

    def by_block(line):
        return jnp.concatenate(
            [line[:, i * BLOCK : (i + 1) * BLOCK] for i in range(blocks)], axis=0
        )

    def pick(array, index):
        line = lax.broadcasted_iota(jnp.int32, array.shape, 0)
        return jnp.sum(jnp.where(index == line, array, 0.0), axis=0, keepdims=True)

    def block_rows(r):
        return pl.ds(pl.multiple_of(r * BLOCK, BLOCK), BLOCK)

    def recur(q):
        place = pl.ds(pl.multiple_of(q * 2 * tokens, 2 * tokens), 2 * tokens)
        gates = lax.dot_general(
            gate_rows[...],
            normed[place, :],
            (((1,), (1,)), ((), ())),
            preferred_element_type=jnp.float32,
        )
        for hh in range(heads):
            head = c * heads + hh
            entry = by_block(pick(gates, head))
            forget = by_block(pick(gates, tp_heads + head)) + bias_ref[head]
            shift = by_block(
                jnp.concatenate([pick(shifts_ref[q * 2 + j], head) for j in range(2)], axis=1)
            )
            logs = jnp.minimum(forget, 0.0) - jnp.log1p(jnp.exp(-jnp.abs(forget))) + shift
            cumulative = jnp.dot(
                logs, upto, precision=HIGHEST, preferred_element_type=jnp.float32
            )
            u = entry - cumulative
            top = jnp.broadcast_to(jnp.max(u, axis=1, keepdims=True), u.shape)
            last = jnp.broadcast_to(cumulative[:, BLOCK - 1 :], u.shape)
            for i in range(blocks):
                u_ref[hh, q * blocks + i] = u[i : i + 1]
                top_ref[hh, q * blocks + i] = top[i : i + 1]
                last_ref[hh, q * blocks + i] = last[i : i + 1]
        for hh in range(heads):
            final_state[q, hh] = jnp.zeros((DK, DV), jnp.float32)

        def scan(i, carry):
            r = q * blocks + i
            keys = proj[0, block_rows(r), k_at : k_at + kq].astype(jnp.float32).T
            keys_t[r] = keys.astype(jnp.bfloat16)
            out = []
            for hh, (m, total) in enumerate(carry):
                last = last_ref[hh, r]
                state = final_state[q, hh]
                states[hh, r] = state
                stable[hh, r] = m
                decayed[hh, r] = total
                peak = jnp.maximum(m, top_ref[hh, r])
                weight = jnp.exp(u_ref[hh, r] - peak) * scale
                weighted = (keys[hh * DK : (hh + 1) * DK] * weight).astype(jnp.bfloat16)
                values = proj[0, block_rows(r), v_at + hh * DV : v_at + (hh + 1) * DV]
                final_state[q, hh] = jnp.exp(m - peak) * state + jnp.dot(
                    weighted, values, preferred_element_type=jnp.float32
                )
                out.append((last + peak, total + last))
            return tuple(out)

        start = tuple(
            (jnp.full((1, BLOCK), EMPTY_LOG, jnp.float32), jnp.zeros((1, BLOCK), jnp.float32))
            for _ in range(heads)
        )
        ended = lax.fori_loop(0, blocks, scan, start)
        for hh, (m, total) in enumerate(ended):
            peak = jnp.maximum(m, total)
            final_state[q, hh] = jnp.exp(m - peak) * final_state[q, hh]
            final_log[q, hh : hh + 1, :] = peak
        send(("state", len(send.copies)), final_state.at[q], came_state.at[q], at.zn[2])
        send(("log", len(send.copies)), final_log.at[q], came_log.at[q], at.zn[2])
        return list(send.copies)[-2:]

    later = at.h == 1
    head_gain = head_gain_ref[:, pl.ds(pl.multiple_of(c * kv, kv), kv)]
    nothing = jnp.zeros((DK, BLOCK), jnp.bfloat16)

    def only(hh, value):
        return jnp.concatenate([value if h == hh else nothing for h in range(heads)], axis=0)

    def cell(b, q):
        def one(i, carry):
            r = b * per + i
            queries = proj[0, block_rows(r), q_at : q_at + kq]
            right, carried = [], []
            for hh in range(heads):
                right.append(only(hh, keys_t[r, hh * DK : (hh + 1) * DK, :]))
            for hh in range(heads):
                m = stable[hh, r]
                m_in = decayed[hh, r] + jnp.where(later, came_log[q, hh : hh + 1, :], 0.0)
                peak = jnp.maximum(m, m_in)
                state = jnp.exp(m - peak) * states[hh, r] + jnp.exp(m_in - peak) * jnp.where(
                    later, came_state[q, hh], 0.0
                )
                right.append(only(hh, state.astype(jnp.bfloat16)))
                carried.append(peak)
            product = jnp.dot(
                queries, jnp.concatenate(right, axis=1), preferred_element_type=jnp.float32
            )
            for hh in range(heads):
                u = jnp.where(causal, u_ref[hh, r], EMPTY_LOG)
                peak = jnp.maximum(jnp.max(u, axis=1, keepdims=True), carried[hh])
                weighted = product[:, hh * BLOCK : (hh + 1) * BLOCK] * scale * jnp.exp(u - peak)
                values = proj[0, block_rows(r), v_at + hh * DV : v_at + (hh + 1) * DV]
                numerator = jnp.dot(
                    weighted.astype(jnp.bfloat16), values, preferred_element_type=jnp.float32
                )
                inter = product[:, heads * BLOCK + hh * DV : heads * BLOCK + (hh + 1) * DV]
                numerator = numerator + jnp.exp(carried[hh] - peak) * inter
                mean = jnp.mean(numerator * numerator, axis=1, keepdims=True)
                lanes_h = slice(hh * DV, (hh + 1) * DV)
                held[block_rows(r), lanes_h] = (
                    numerator * lax.rsqrt(mean + EPSILON) * head_gain[:, lanes_h]
                )
            return carry

        lax.fori_loop(0, per, one, 0)

    edge = entered.shape[1] - blocks * BLOCK

    def enter(q):
        def one(i, carry):
            rows = block_rows(q * blocks + i)
            value = proj[1, rows, 0:conv].astype(jnp.float32) * proj[
                1, rows, conv : 2 * conv
            ].astype(jnp.float32)
            value = value.astype(jnp.bfloat16).astype(jnp.float32)
            entered[q, pl.ds(pl.multiple_of(edge + i * BLOCK, edge), BLOCK), :] = value
            return carry

        lax.fori_loop(0, blocks, one, 0)
        rim[q] = entered[q, blocks * BLOCK : blocks * BLOCK + edge, :].astype(jnp.bfloat16)

    def respond():
        taps = taps_ref[:, pl.ds(pl.multiple_of(c * conv, conv), conv)]
        for q in range(2):
            before = came_rim[q].astype(jnp.float32)
            entered[q, 0:edge, :] = jnp.where(later, before, 0.0)
            for i in range(blocks):
                first = edge + i * BLOCK - (KERNEL - 1)
                response = taps[0:1] * entered[q, first : first + BLOCK, :]
                for tap in range(1, KERNEL):
                    response = response + taps[tap : tap + 1] * entered[
                        q, first + tap : first + tap + BLOCK, :
                    ]
                start = (q * blocks + i) * BLOCK
                held[start : start + BLOCK, kv : kv + conv] = response

    def close(b):
        project(b, 2)

        def one(i, carry):
            rows = block_rows(b * per + i)
            opened = jax.nn.sigmoid(proj[2, rows, 0:kv].astype(jnp.float32))
            both[t, b, block_rows(i), 0:kv] = (held[rows, 0:kv] * opened).astype(jnp.bfloat16)
            value = proj[2, rows, kv : kv + conv].astype(jnp.float32) * held[rows, kv : kv + conv]
            both[t, b, block_rows(i), kv : kv + conv] = value.astype(jnp.bfloat16)
            return carry

        lax.fori_loop(0, per, one, 0)

    for b in (mine, by_z):
        project(b, 0)
    send.arrived(("x same", 2))
    to_y(1, 2)
    send.arrived(("x other", 2))
    to_z(1, 2)
    forward(0, 2)
    came_own = recur(x)
    project(by_x, 0)
    forward(1, 1)
    merge_to_z(0)
    merge_to_y(0)
    for name in came_own:
        send.arrived(name)
    cell(mine, x)
    cell(by_z, x)
    send.arrived("x tok on")
    send("t zx", tok.at[by_both, t], tok.at[by_both, t], at.tn)
    send.arrived("x shift")
    send.arrived("x shift on")
    forward(1, 2)
    for s in range(1, MERGE_SLICES):
        merge_to_z(s)
        merge_to_y(s)
    send.arrived("t zx")
    normalize(by_both)
    project(by_both, 0)
    came_other = recur(other_x)
    all_here(1)
    for b in (mine, by_z):
        project(b, 1)
    forward_merge(0)
    for b in (by_x, by_both):
        project(b, 1)
    for q in range(2):
        enter(q)
    send("rim", rim, came_rim, at.zn[2])
    for name in came_other:
        send.arrived(name)
    for s in range(1, MERGE_SLICES):
        forward_merge(s)
    cell(by_both, other_x)
    cell(by_x, other_x)
    send.arrived("rim")
    respond()
    all_here(2)

    columns = out_ref.shape[1]
    rows_half = tokens // 2

    def merge(b, part, s):
        rows = pl.ds(part * rows_half, rows_half)
        place = pl.ds(s * out_strip, out_strip)
        total = None
        for side in range(2):
            for group, (start, width) in enumerate(((0, kv), (kv, conv))):
                product = jnp.dot(
                    both[side, b, rows, start : start + width],
                    pieces[group * 2 + side, :, place],
                    preferred_element_type=jnp.float32,
                )
                total = product if total is None else total + product
        return total

    def pass_on(name, s, index, b, part, peer, extra=None):
        rows = pl.ds(part * rows_half, rows_half)
        place = pl.ds(s * out_strip, out_strip)
        total = merge(b, part, s)
        if extra is not None:
            total = total + relayed[extra, :, place].astype(jnp.float32)
        partial[index, rows, place] = total.astype(jnp.bfloat16)
        target = relayed.at[part, :, place] if index == 2 else came.at[index, rows, place]
        send((name, s), partial.at[index, rows, place], target, peer)

    def swap(step, b):
        close(b)
        send(("t", step), both.at[t, b], both.at[t, b], at.tn)

    for step, b in enumerate((by_both, by_x, by_z, mine)):
        swap(step, b)
    for s in range(MERGE_SLICES):
        for k in range(4):
            send.arrived(("my", k, s))
        for step in range(3 if s == 0 else 0):
            send.arrived(("t", step))
        pass_on("sum d0", s, 2, by_both, 0, at.xn)
        pass_on("sum d1", s, 2, by_both, 1, at.zn[1])
        pass_on("sum x0", s, 0, by_x, 0, at.xn)
        pass_on("sum z1", s, 1, by_z, 1, at.zn[1])
    send.arrived(("t", 3))
    for s in range(MERGE_SLICES):
        send.arrived(("sum d0", s))
        pass_on("sum z0", s, 1, by_z, 0, at.zn[1], 0)
        send.arrived(("sum d1", s))
        pass_on("sum x1", s, 0, by_x, 1, at.xn, 1)
        for part in range(2):
            place = pl.ds(s * out_strip, out_strip)
            own_sum[pl.ds(part * rows_half, rows_half), place] = merge(mine, part, s)
    for s in range(MERGE_SLICES):
        for part, names in ((0, ("sum x0", "sum z0")), (1, ("sum z1", "sum x1"))):
            for name in names:
                send.arrived((name, s))
            rows = slice(part * rows_half, (part + 1) * rows_half)
            place = slice(s * out_strip, (s + 1) * out_strip)
            total = own_sum[rows, place] + came[0, rows, place].astype(jnp.float32)
            total = total + came[1, rows, place].astype(jnp.float32)
            out_ref[rows, place] = total.astype(jnp.bfloat16)
    send.drain()


def layer(gain, tokens, shift, gate_rows, bias, head_gain, taps, merge, heads, grouped):
    weights = sum(grouped, [])
    rows, width_t = tokens.shape
    columns = merge.shape[1]
    features = 2 * width_t
    depth = weights[0].shape[0]
    groups = [[w.shape[1] // 4 for w in group] for group in grouped]
    broad = sum(groups[0])
    gates = gate_rows.shape[0]
    kv, conv, m_depth = heads * DV, groups[1][0], merge.shape[0]
    blocks = 4 * rows // BLOCK
    vmem = pl.BlockSpec(memory_space=pltpu.VMEM)
    hbm = pl.BlockSpec(memory_space=pl.ANY)
    smem = pl.BlockSpec(memory_space=pltpu.SMEM)
    f32, bf16 = jnp.float32, jnp.bfloat16
    return pl.pallas_call(
        lambda *refs: layer_kernel(heads, groups, *refs),
        out_shape=jax.ShapeDtypeStruct((rows, columns), bf16),
        in_specs=[vmem, hbm, hbm, hbm, smem, vmem, vmem, hbm] + [hbm] * len(weights),
        out_specs=vmem,
        scratch_shapes=[
            pltpu.VMEM((4, 2, rows, width_t), bf16),
            pltpu.VMEM((4 * rows, features), bf16),
            pltpu.VMEM((4, len(groups), depth, broad), bf16),
            pltpu.VMEM((len(groups), depth, broad), bf16),
            pltpu.VMEM((len(groups), features, broad), bf16),
            pltpu.VMEM((gates, features), bf16),
            pltpu.VMEM((4,) + shift.shape, f32),
            pltpu.VMEM((len(groups), 4 * rows, broad), bf16),
            pltpu.VMEM((2, m_depth // 2, columns), bf16),
            pltpu.VMEM((4, m_depth, columns), bf16),
            pltpu.VMEM((2, 4, rows, kv + conv), bf16),
            pltpu.VMEM((2, 16 + 2 * rows, conv), f32),
            pltpu.VMEM((4 * rows, kv + conv), f32),
            pltpu.VMEM((blocks, heads * DK, BLOCK), bf16),
            pltpu.VMEM((heads, blocks, 1, BLOCK), f32),
            pltpu.VMEM((heads, blocks, 1, BLOCK), f32),
            pltpu.VMEM((heads, blocks, 1, BLOCK), f32),
            pltpu.VMEM((heads, blocks, DK, DV), f32),
            pltpu.VMEM((heads, blocks, 1, BLOCK), f32),
            pltpu.VMEM((heads, blocks, 1, BLOCK), f32),
            pltpu.VMEM((2, heads, DK, DV), f32),
            pltpu.VMEM((2, heads, BLOCK), f32),
            pltpu.VMEM((2, heads, DK, DV), f32),
            pltpu.VMEM((2, heads, BLOCK), f32),
            pltpu.VMEM((2, 16, conv), bf16),
            pltpu.VMEM((2, 16, conv), bf16),
            pltpu.VMEM((rows, columns), f32),
            pltpu.VMEM((3, rows, columns), bf16),
            pltpu.VMEM((2, rows, columns), bf16),
            pltpu.VMEM((2, rows // 2, columns), bf16),
            pltpu.SemaphoreType.DMA((4 + 4 * len(weights),)),
            pltpu.SemaphoreType.DMA((112,)),
            pltpu.SemaphoreType.DMA((112,)),
        ],
        compiler_params=pltpu.CompilerParams(
            collective_id=0, has_side_effects=True, vmem_limit_bytes=67043328
        ),
        cost_estimate=pl.CostEstimate(
            flops=8 * rows * features * broad * len(groups), bytes_accessed=0, transcendentals=0
        ),
        name="layer",
    )(gain, tokens, shift, gate_rows, bias, head_gain, taps, merge, *weights)


def regrouped(
    tokens,
    norm_gain,
    query_weight,
    key_weight,
    value_weight,
    outgate_weight,
    gate_weight,
    forget_bias,
    forget_shift,
    head_norm_gain,
    exit_weight,
    entry_weight,
    signal_weight,
    conv_kernel,
    merge_weight,
):
    grouped = [
        [query_weight, key_weight, value_weight],
        [entry_weight, signal_weight],
        [outgate_weight, exit_weight],
    ]
    heads = gate_weight.shape[2] // 4
    gate_rows = gate_weight.reshape(gate_weight.shape[0], -1).T
    mixed = layer(
        norm_gain[None],
        tokens[0],
        forget_shift[0],
        gate_rows,
        forget_bias,
        head_norm_gain[None],
        conv_kernel,
        merge_weight,
        heads,
        grouped,
    )
    return mixed[None]


def solution(mesh):
    placed = (
        P("fs", "sp", "tp"),
        P(),
        P(("sp", "fs"), "tp"),
        P(("sp", "fs"), "tp"),
        P(("sp", "fs"), "tp"),
        P(("sp", "fs"), "tp"),
        P(("sp", "fs"), None, "tp"),
        P("tp"),
        P("fs", "tp", "sp"),
        P("tp"),
        P(("sp", "fs"), "tp"),
        P(("sp", "fs"), "tp"),
        P(("sp", "fs"), "tp"),
        P(None, "tp"),
        P(("sp", "fs"), "tp"),
    )
    sp, tp = mesh.shape["sp"], mesh.shape["tp"]

    def step(*args):
        square = (sp, mesh.shape["fs"], tp) == (4, 4, 2)
        body = regrouped if square else local
        return jax.shard_map(
            body, mesh=mesh, in_specs=placed, out_specs=P("fs", "sp", "tp"), check_vma=False
        )(*args)

    return step
```

time: 347 us -> 165 us (0.48)
  the two profiles are of different devices: /device:TPU:9 before, /device:TPU:0 now
where the time goes in v1:
time: 165 us
  Pallas kernels  162 us (98%)
  local copies, waits for them, and re-layouts  2.26 us (1%)
    pallas_call x1, Pallas kernels, layer(): pl.pallas_call(lambda *refs: layer_kernel(heads, groups, *refs), out_shap...  162 us

profile of v1, /device:TPU:0, one launch (start us, length us, event | category | flops | bytes accessed | tf_op | source)
XLA Modules:
  0.0 164.7 jit_solution(5390907681163045789)
XLA Ops:
  0.0 162.4 %layer.1 = bf16[512,1024]{1,0:T(8,128)(2,1)} custom-call(f32[1,2048]{1,0:T(1,128)} %bitcast.11, bf16[512,1024]{1,0:T(8,128)(2,1)} %bitcast.9, f32[8,512]{1,0:T(8,128)} %bitcast.10, bf16[16,128]{1,0:T(8,128)(2,1)} %bitcast.12, f32[8]{0:T(128)} %refs_4_.1, f32[1,1024]{1,0:T(1,128)} %bitcast.13, f32[3,1024]{1,0:T(4,128)} %refs_6_.1, bf16[256,1024]{1,0:T(8,128)(2,1)} %refs_7_.1, ...), custom_call_target="tpu_custom_call" | custom-call | flops 12884901888 | tf_op jit(solution)/shard_map/layer/pallas_call | solution.py:801
  162.5 2.3 %copy.17 = bf16[1,512,1024]{2,1,0:T(8,128)(2,1)} copy(bf16[1,512,1024]{2,1,0:T(8,128)(2,1)} %bitcast.8) | data formatting | bytes 2097152
